TPU v7x, 32 devices: a whole 2x2x4 slice. The times are simulated.
32 devices in a mesh: kv: 8 (over z, y), tp: 4 (over x, core).
Axes of the slice: x: 2, y: 2, z: 4, core: 2. Of those that a mesh axis runs over, the one named last changes fastest.
Arguments:
- stream: bfloat16 [24, 4096], P(None, ('kv', 'tp')), may hold values from -50 to 50
- attention_gain: float32 [4096], P(('kv', 'tp')), may hold values from 0.1 to 1.9
- query_down: bfloat16 [4096, 1536], P(('kv', 'tp')), may hold values from -0.09375 to 0.09375
- latent_down: bfloat16 [4096, 512], P(('kv', 'tp')), may hold values from -0.09375 to 0.09375
- rotary_down: bfloat16 [4096, 64], P(('kv', 'tp')), may hold values from -0.1875 to 0.1875
- query_gain: float32 [1536], replicated, may hold values from 0.1 to 1.9
- latent_gain: float32 [512], replicated, may hold values from 0.1 to 1.9
- query_content: bfloat16 [1536, 2048], P(None, 'tp'), may hold values from -0.15625 to 0.15625
- query_rotary: bfloat16 [1536, 1024], P(None, 'tp'), may hold values from -0.15625 to 0.15625
- key_absorb: bfloat16 [16, 128, 512], P('tp'), may hold values from -0.5 to 0.5
- value_absorb: bfloat16 [16, 512, 128], P('tp'), may hold values from -0.25 to 0.25
- latent_cache: bfloat16 [24, 2048, 512], P(None, 'kv'), may hold values from -1200 to 1200
- rotary_cache: bfloat16 [24, 2048, 64], P(None, 'kv'), may hold values from -5 to 5
- head_gain: float32 [2048], P('tp'), may hold values from 0.1 to 1.9
- output_weight: bfloat16 [2048, 4096], P('tp', 'kv'), may hold values from -0.125 to 0.125
- mixer_gain: float32 [4096], P('kv'), may hold values from 0.1 to 1.9
- gate_weight: bfloat16 [4096, 11264], P('kv', 'tp'), may hold values from -0.09375 to 0.09375
- up_weight: bfloat16 [4096, 11264], P('kv', 'tp'), may hold values from -0.09375 to 0.09375
- down_weight: bfloat16 [11264, 4096], P('tp', 'kv'), may hold values from -0.0546875 to 0.0546875
Outputs:
- stream_out: bfloat16 [24, 4096], P(None, ('kv', 'tp'))
All inputs are finite; a program needn't handle non-finite values.
Results may differ from a plain program's by a relative error of at most 0.018.
Values may be sent and summed in bfloat16 or wider, within the bound.
A program may use at most 64 MiB of HBM per device.

v0:
```python
import jax
import jax.numpy as jnp
from jax import lax
from jax.sharding import PartitionSpec as P

epsilon = 1e-06
rope_base = 10000.0


def rotate(values, position):
    half = values.shape[-1] // 2
    freqs = rope_base ** (-jnp.arange(half, dtype=jnp.float32) * 2.0 / values.shape[-1])
    angle = position * freqs
    cosine = jnp.cos(angle)
    sine = jnp.sin(angle)
    first = values[..., :half]
    second = values[..., half:]
    return jnp.concatenate(
        [first * cosine - second * sine, second * cosine + first * sine], axis=-1
    )


def inv_rms(values):
    return lax.rsqrt(jnp.mean(values * values, axis=-1) + epsilon)


def sum_squares(values):
    return jnp.sum(values * values, axis=-1)


def matmul(left, right):
    return jnp.dot(left, right, preferred_element_type=jnp.float32)


def local(
    stream,
    attention_gain,
    query_down,
    latent_down,
    rotary_down,
    query_gain,
    latent_gain,
    query_content,
    query_rotary,
    key_absorb,
    value_absorb,
    latent_cache,
    rotary_cache,
    head_gain,
    output_weight,
    mixer_gain,
    gate_weight,
    up_weight,
    down_weight,
):
    kv_count = lax.axis_size("kv")
    tp_count = lax.axis_size("tp")
    batch_rows = stream.shape[0]
    model_width = stream.shape[1] * kv_count * tp_count
    position = jnp.float32(latent_cache.shape[1] * kv_count)
    stream_block = lax.all_gather(stream, "tp", axis=1, tiled=True)
    stream_f = stream.astype(jnp.float32)
    first_scaled = (stream_f * attention_gain).astype(jnp.bfloat16)
    query_sum, latent_sum, rotary_sum, square_sum = lax.psum(
        (
            matmul(first_scaled, query_down),
            matmul(first_scaled, latent_down),
            matmul(first_scaled, rotary_down),
            sum_squares(stream_f),
        ),
        ("kv", "tp"),
    )
    first_scale = lax.rsqrt(square_sum / model_width + epsilon)[:, None]
    query_low = first_scale * query_sum
    latent_new = first_scale * latent_sum
    rotary_new = first_scale * rotary_sum
    query_normed = (query_low * inv_rms(query_low)[:, None] * query_gain).astype(jnp.bfloat16)
    latent_row = (latent_new * inv_rms(latent_new)[:, None] * latent_gain).astype(jnp.bfloat16)
    rotary_row = rotate(rotary_new, position).astype(jnp.bfloat16)
    heads_here = key_absorb.shape[0]
    query_plain = matmul(query_normed, query_content).astype(jnp.bfloat16)
    query_plain = query_plain.reshape(batch_rows, heads_here, key_absorb.shape[1])
    query_turned = matmul(query_normed, query_rotary).reshape(
        batch_rows, heads_here, rotary_cache.shape[2]
    )
    query_turned = rotate(query_turned, position).astype(jnp.bfloat16)
    query_latent = jnp.einsum(
        "bhn,hnc->bhc", query_plain, key_absorb, preferred_element_type=jnp.float32
    ).astype(jnp.bfloat16)
    scale = (key_absorb.shape[1] + rotary_cache.shape[2]) ** (-0.5)
    scores = (
        jnp.einsum("bhc,bpc->bhp", query_latent, latent_cache, preferred_element_type=jnp.float32)
        + jnp.einsum("bhr,bpr->bhp", query_turned, rotary_cache, preferred_element_type=jnp.float32)
    ) * scale
    maxima = jnp.max(scores, axis=-1)
    expo = jnp.exp(scores - maxima[..., None])
    totals = jnp.sum(expo, axis=-1)
    weighted = jnp.einsum(
        "bhp,bpc->bhc", expo.astype(jnp.bfloat16), latent_cache, preferred_element_type=jnp.float32
    ).astype(jnp.bfloat16)
    all_maxima, all_totals = (
        lax.all_gather(maxima[None], "kv", axis=0, tiled=True),
        lax.all_gather(totals[None], "kv", axis=0, tiled=True),
    )
    own_score = (
        jnp.sum(
            query_latent.astype(jnp.float32) * latent_row.astype(jnp.float32)[:, None, :], axis=-1
        )
        + jnp.sum(
            query_turned.astype(jnp.float32) * rotary_row.astype(jnp.float32)[:, None, :], axis=-1
        )
    ) * scale
    largest = jnp.maximum(jnp.max(all_maxima, axis=0), own_score)
    factors = jnp.exp(all_maxima - largest[None])
    own_weight = jnp.exp(own_score - largest)
    denominator = jnp.sum(factors * all_totals, axis=0) + own_weight
    merged = jnp.sum(
        factors[..., None]
        * lax.all_gather(weighted[None], "kv", axis=0, tiled=True).astype(jnp.float32),
        axis=0,
    )
    merged = merged + own_weight[..., None] * latent_row.astype(jnp.float32)[:, None, :]
    latent_mix = (merged / denominator[..., None]).astype(jnp.bfloat16)
    head_values = jnp.einsum(
        "bhc,hcv->bhv", latent_mix, value_absorb, preferred_element_type=jnp.float32
    ).astype(jnp.bfloat16)
    head_f = head_values.reshape(batch_rows, heads_here * value_absorb.shape[2]).astype(jnp.float32)
    head_square = lax.psum(sum_squares(head_f), "tp")
    head_scale = lax.rsqrt(head_square / (head_f.shape[1] * tp_count) + epsilon)[:, None]
    head_scaled = (head_f * head_gain).astype(jnp.bfloat16)
    attended = lax.psum(matmul(head_scaled, output_weight).astype(jnp.bfloat16), "tp").astype(
        jnp.float32
    )
    middle = (stream_block.astype(jnp.float32) + head_scale * attended).astype(jnp.bfloat16)
    middle_f = middle.astype(jnp.float32)
    second_scaled = (middle_f * mixer_gain).astype(jnp.bfloat16)
    gate_part = matmul(second_scaled, gate_weight)
    up_part = matmul(second_scaled, up_weight)
    gate_total, up_total, middle_square = (
        lax.psum(gate_part.astype(jnp.bfloat16), "kv").astype(jnp.float32),
        lax.psum(up_part.astype(jnp.bfloat16), "kv").astype(jnp.float32),
        lax.psum(sum_squares(middle_f).astype(jnp.bfloat16), "kv").astype(jnp.float32),
    )
    second_scale = lax.rsqrt(middle_square / model_width + epsilon)[:, None]
    hidden = (jax.nn.silu(second_scale * gate_total) * (second_scale * up_total)).astype(
        jnp.bfloat16
    )
    mixed = lax.psum_scatter(
        matmul(hidden, down_weight).astype(jnp.bfloat16), "tp", scatter_dimension=1, tiled=True
    ).astype(jnp.float32)
    share_width = mixed.shape[1]
    own_middle = lax.dynamic_slice_in_dim(
        middle_f, lax.axis_index("tp") * share_width, share_width, 1
    )
    return (own_middle + mixed).astype(jnp.bfloat16)


def solution(mesh):
    return jax.shard_map(
        local,
        mesh=mesh,
        in_specs=(
            P(None, ("kv", "tp")),
            P(("kv", "tp")),
            P(("kv", "tp"), None),
            P(("kv", "tp"), None),
            P(("kv", "tp"), None),
            P(),
            P(),
            P(None, "tp"),
            P(None, "tp"),
            P("tp", None, None),
            P("tp", None, None),
            P(None, "kv", None),
            P(None, "kv", None),
            P("tp"),
            P("tp", "kv"),
            P("kv"),
            P("kv", "tp"),
            P("kv", "tp"),
            P("tp", "kv"),
        ),
        out_specs=P(None, ("kv", "tp")),
        check_vma=False,
    )
```

profile of v0, /device:TPU:0, one launch (start us, length us, event | category | flops | bytes accessed | tf_op | source)
XLA Modules:
  0.0 365.7 jit_solution(8575871033755606622)
XLA Ops:
  6.5 2.0 fusion.32
  8.6 0.8 fusion.26
  10.0 1.1 fusion.30
  11.1 0.9 fusion.28
  12.0 8.0 %all_gather.12 = bf16[24,512]{1,0:T(8,128)(2,1)} all-gather(bf16[24,128]{1,0:T(8,128)(2,1)} %param.19), channel_id=1, replica_groups=mesh['kv'=8,'tp'=4] {'tp'}, dimensions={1}, use_global_device_ids=true | all-gather | bytes 30720 | tf_op jit(solution)/shard_map/all_gather | solution.py:61
  20.0 40.5 %all-reduce = (f32[24]{0:T(128)S(1)}, f32[24,512]{1,0:T(8,128)S(1)}, f32[24,64]{1,0:T(8,128)S(1)}) all-reduce(f32[24]{0:T(128)S(1)} %fusion.26, f32[24,512]{1,0:T(8,128)S(1)} %fusion.30, f32[24,64]{1,0:T(8,128)S(1)} %fusion.28), channel_id=1, replica_groups=mesh['kv'=8,'tp'=4] {'kv','tp'}, use_global_device_ids=true, to_apply=%region_1.0 | all-reduce | flops 13848 | bytes 110784 | tf_op jit(solution)/shard_map/psum | solution.py:64
  60.8 0.8 fusion.20
  63.0 75.0 %all-reduce.5.cloned.1.call-done = f32[24,1536]{1,0:T(8,128)} async-done(((f32[24,1536]{1,0:T(8,128)}), f32[24,1536]{1,0:T(8,128)}) %all-reduce.5.cloned.1.call-update) | async-done | bytes 147472 | tf_op jit(solution)/shard_map/psum | solution.py:64
  137.9 1.1 multiply_reduce_fusion.1
  139.1 1.5 fusion.38
  140.7 0.7 subtract_convert_fusion
  141.4 1.9 fusion.4
  143.6 4.6 %fusion.10 = f32[24,4,256]{2,1,0:T(4,128)S(1)} fusion(bf16[24,256,512]{2,1,0:T(8,128)(2,1)} %param.30, bf16[24,4,512]{2,0,1:T(8,128)(2,1)S(1)} %get-tuple-element.23), kind=kOutput, calls=%fused_computation.24 | convolution fusion | flops 25165824 | bytes 6488064 | tf_op jit(solution)/shard_map/bhc,bpc->bhp/dot_general | solution.py:92
  148.7 0.8 fusion.15
  149.4 4.4 %convolution_convert_fusion.2 = bf16[24,4,512]{2,1,0:T(4,128)(2,1)} fusion(bf16[24,256,512]{2,1,0:T(8,128)(2,1)} %param.30, f32[24,4,256]{2,1,0:T(4,128)S(1)} %get-tuple-element.21, f32[24,4]{1,0:T(8,128)S(1)} %get-tuple-element.20), kind=kOutput, calls=%fused_computation.4 | convolution fusion | flops 25264128 | bytes 6488448 | tf_op jit(solution)/shard_map/bhp,bpc->bhc/dot_general | solution.py:98
  153.8 28.4 %all-gather.3 = f32[8,24,4]{1,2,0:T(4,128)S(1)} all-gather(f32[1,24,4]{1,2,0:T(4,128)S(1)} %bitcast.42), channel_id=2, replica_groups=mesh['kv'=8,'tp'=4] {'kv'}, dimensions={0}, use_global_device_ids=true | all-gather | bytes 3456 | tf_op jit(solution)/shard_map/all_gather | solution.py:102
  182.5 0.8 copy.45
  183.3 26.1 %all-gather.4 = f32[8,24,4]{1,2,0:T(4,128)S(1)} all-gather(f32[1,24,4]{1,2,0:T(4,128)S(1)} %bitcast.43), channel_id=4, replica_groups=mesh['kv'=8,'tp'=4] {'kv'}, dimensions={0}, use_global_device_ids=true | all-gather | bytes 3456 | tf_op jit(solution)/shard_map/all_gather | solution.py:103
  210.6 0.8 copy.43
  211.5 32.5 %all-gather.1 = bf16[192,4,512]{2,1,0:T(4,128)(2,1)S(1)} all-gather(bf16[24,4,512]{2,1,0:T(4,128)(2,1)} %convolution_convert_fusion.2), channel_id=3, replica_groups=mesh['kv'=8,'tp'=4] {'kv'}, dimensions={0}, use_global_device_ids=true | all-gather | bytes 884736 | tf_op jit(solution)/shard_map/all_gather | solution.py:119
  244.5 1.4 multiply_reduce_fusion.3
  246.1 10.3 %psum.68 = bf16[24,512]{1,0:T(8,128)(2,1)S(1)} all-reduce(bf16[24,512]{1,0:T(8,128)(2,1)S(1)} %convolution_convert_fusion.6), channel_id=1, replica_groups=mesh['kv'=8,'tp'=4] {'tp'}, use_global_device_ids=true, to_apply=%region_16.0 | all-reduce | flops 12288 | bytes 49152 | tf_op jit(solution)/shard_map/psum | solution.py:131
  256.4 6.3 %psum.67 = f32[24]{0:T(128)S(1)} all-reduce(f32[24]{0:T(128)S(1)} %get-tuple-element.24), channel_id=1, replica_groups=mesh['kv'=8,'tp'=4] {'tp'}, use_global_device_ids=true, to_apply=%region_15.0 | all-reduce | flops 24 | bytes 192 | tf_op jit(solution)/shard_map/psum | solution.py:128
  262.7 1.1 multiply_reduce_fusion.2
  263.8 1.8 convolution_convert_fusion
  265.6 1.1 convolution_convert_fusion.1
  266.8 18.2 %psum.69 = bf16[24]{0:T(256)(128)(2,1)S(1)} all-reduce(bf16[24]{0:T(256)(128)(2,1)S(1)} %get-tuple-element.10), channel_id=1, replica_groups=mesh['kv'=8,'tp'=4] {'kv'}, use_global_device_ids=true, to_apply=%region_18.0 | all-reduce | flops 24 | bytes 96 | tf_op jit(solution)/shard_map/psum | solution.py:142
  285.0 50.3 %all-reduce.7.cloned.1.call-done = (bf16[24,2816]{1,0:T(8,128)(2,1)}, bf16[24,2816]{1,0:T(8,128)(2,1)}) async-done(((bf16[24,2816]{1,0:T(8,128)(2,1)}, bf16[24,2816]{1,0:T(8,128)(2,1)}), (bf16[24,2816]{1,0:T(8,128)(2,1)}, bf16[24,2816]{1,0:T(8,128)(2,1)})) %all-reduce.7.cloned.1.call-update) | async-done | bytes 270352 | tf_op jit(solution)/shard_map/psum | solution.py:141
  335.3 2.5 convolution_convert_fusion.5
  337.9 0.7 copy.47
  338.6 19.1 %reduce-scatter.4.cloned.1.call-done = bf16[128,24]{1,0:T(8,128)(2,1)} async-done(((bf16[512,24]{1,0:T(8,128)(2,1)}), bf16[128,24]{1,0:T(8,128)(2,1)}) %reduce-scatter.4.cloned.1.call-update) | async-done | bytes 6160
  357.7 0.8 copy.48
  (49 shorter events, 6.1 us)
Async XLA Ops:
  6.5 257.2 %copy-start = (bf16[512,2816]{1,0:T(8,128)(2,1)S(1)}, bf16[512,2816]{1,0:T(8,128)(2,1)}, u32[]{:S(2)}) copy-start(bf16[512,2816]{1,0:T(8,128)(2,1)} %param.36) | copy-start | bytes 8650756
  6.5 136.8 %copy-start.4 = (bf16[4,128,512]{2,1,0:T(8,128)(2,1)S(1)}, bf16[4,128,512]{2,1,0:T(8,128)(2,1)}, u32[]{:S(2)}) copy-start(bf16[4,128,512]{2,1,0:T(8,128)(2,1)} %param.28) | copy-start | bytes 1572868
  6.5 131.4 %all-reduce.5.cloned.1.call-start = ((), (), s32[]{:S(2)}) async-start(), calls=%async_computation.1 | async-start | bytes 294912 | tf_op jit(solution)/shard_map/psum | solution.py:64
  8.6 326.8 %all-reduce.7.cloned.1.call-start = ((), (), s32[]{:S(2)}) async-start(), calls=%async_computation.3 | async-start | bytes 540672 | tf_op jit(solution)/shard_map/psum | solution.py:141
  60.5 80.1 %copy-start.6 = (f32[24]{0:T(128)}, f32[24]{0:T(128)S(1)}, u32[]{:S(2)}) copy-start(f32[24]{0:T(128)S(1)} %add_rsqrt_fusion.4) | copy-start | bytes 292
  139.1 1.5 copy-start.9
  143.6 4.6 %copy-start.2 = (bf16[24,256,64]{1,2,0:T(8,128)(2,1)S(1)}, bf16[24,256,64]{1,2,0:T(8,128)(2,1)}, u32[]{:S(2)}) copy-start(bf16[24,256,64]{1,2,0:T(8,128)(2,1)} %param.31) | copy-start | bytes 2359300
  149.4 32.8 %copy-start.5 = (f32[24,64]{1,0:T(8,128)S(1)}, f32[24,64]{1,0:T(8,128)}, u32[]{:S(2)}) copy-start(f32[24,64]{1,0:T(8,128)} %maximum_convert_fusion) | copy-start | bytes 18436
  153.8 92.1 %copy-start.3 = (bf16[512,512]{1,0:T(8,128)(2,1)S(1)}, bf16[512,512]{1,0:T(8,128)(2,1)}, u32[]{:S(2)}) copy-start(bf16[512,512]{1,0:T(8,128)(2,1)} %param.33) | copy-start | bytes 1572868
  211.5 34.5 %copy-start.8 = (f32[512]{0:T(512)S(1)}, f32[512]{0:T(512)}, u32[]{:S(2)}) copy-start(f32[512]{0:T(512)} %param.32) | copy-start | bytes 6148
  244.5 21.1 %copy-start.7 = (f32[512]{0:T(512)S(1)}, f32[512]{0:T(512)}, u32[]{:S(2)}) copy-start(f32[512]{0:T(512)} %param.34) | copy-start | bytes 6148
  262.7 2.9 copy-start.1
  266.8 90.9 %reduce-scatter.4.cloned.1.call-start = ((), (), s32[]{:S(2)}) async-start(), calls=%async_computation.2 | async-start | bytes 163840
Sparse Core Ops, SparseCore 0:
  12.9 125.0 all-reduce.4
  266.9 68.3 all-reduce.6
  338.8 18.9 reduce-scatter.3
where the time goes:
time: 367 us; the launch traced here: 366 us
  blocking collectives  170 us (46%)
  waiting for transfers between devices  144 us (39%)
  matrix products  24.1 us (7%)
  between operations  13.2 us (4%)
  other arithmetic  10.1 us (3%)
    psum x1, waiting for transfers between devices, local(): lax.psum((matmul(first_scaled, query_down), matmul(first_scaled, latent_d...  75 us
    psum x1, waiting for transfers between devices, local(): lax.psum(up_part.astype(jnp.bfloat16), 'kv').astype(jnp.float32)  50.3 us
    psum x1, blocking collectives, local(): lax.psum((matmul(first_scaled, query_down), matmul(first_scaled, latent_d...  40.5 us
    all_gather x1, blocking collectives, local(): lax.all_gather(weighted[None], 'kv', axis=0, tiled=True).astype(jnp.float32)  32.5 us
    all_gather x1, blocking collectives, local(): lax.all_gather(maxima[None], 'kv', axis=0, tiled=True)  28.4 us
    all_gather x1, blocking collectives, local(): lax.all_gather(totals[None], 'kv', axis=0, tiled=True)  26.1 us
    unnamed x4, waiting for transfers between devices  19.1 us
    psum x1, blocking collectives, local(): lax.psum(sum_squares(middle_f).astype(jnp.bfloat16), 'kv')  18.2 us
  transfers between devices with their start and end apart: 3, of which 3 were waited for; matrix products, arithmetic and copies ran while one was open for 2% of the time, Pallas kernels for 0%

commit v1 on v0

--- a/solution.py
+++ b/solution.py
@@ -1,6 +1,11 @@
+import functools
+
 import jax
 import jax.numpy as jnp
+import numpy as np
 from jax import lax
+from jax.experimental import pallas as pl
+from jax.experimental.pallas import tpu as pltpu
 from jax.sharding import PartitionSpec as P
 
 epsilon = 1e-06
@@ -155,9 +160,624 @@
     return (own_middle + mixed).astype(jnp.bfloat16)
 
 
+LANES = 128
+SUBLANES = 8
+MESH = pl.DeviceIdType.MESH
+
+
+def ceil_div(value, step):
+    return -(-value // step)
+
+
+def tables(width, count, position):
+    half = width // 2
+    freqs = rope_base ** (-np.arange(half, dtype=np.float64) * 2.0 / width)
+    angle = position * freqs
+    cosine = np.concatenate([np.cos(angle), np.cos(angle)])
+    sine = np.concatenate([-np.sin(angle), np.sin(angle)])
+    return (
+        np.tile(cosine, count)[None].astype(np.float32),
+        np.tile(sine, count)[None].astype(np.float32),
+    )
+
+
+def turned(values, cosine, sine, width):
+    lanes = values.shape[1]
+    half = width // 2
+    lane = lax.broadcasted_iota(jnp.int32, values.shape, 1)
+    ahead = pltpu.roll(values, lanes - half, 1)
+    behind = pltpu.roll(values, half, 1)
+    swapped = jnp.where(lax.rem(lane, width) < half, ahead, behind)
+    return values * cosine + swapped * sine
+
+
+def matmul_nt(left, right):
+    return lax.dot_general(
+        left, right, (((1,), (1,)), ((), ())), preferred_element_type=jnp.float32
+    )
+
+
+def fused(
+    n_kv,
+    n_tp,
+    dims,
+    stream_ref,
+    attention_gain,
+    query_gain,
+    latent_gain,
+    head_gain,
+    mixer_gain,
+    cos_ref,
+    sin_ref,
+    *refs,
+):
+    rows, depth, qrank, kvrank, rope, nope, vdim, heads, hidden_width, block_width, share, positions = dims
+    hbm = refs[:13]
+    out_ref = refs[13]
+    vmem = refs[14:27]
+    (
+        load_sems,
+        tp_sems,
+        kv_sems,
+        stream_all,
+        a_send,
+        a_recv,
+        a_sum,
+        a_part,
+        a_total,
+        a_all,
+        q_lat,
+        q_rot,
+        own_lat,
+        own_stat,
+        own_rows,
+        s_ref,
+        e_ref,
+        w_ref,
+        w_send,
+        w_recv,
+        st_send,
+        st_recv,
+        hv_send,
+        hv_recv,
+        hv_rows,
+        o_recv,
+        osq_recv,
+        o_send,
+        osq_send,
+        mid_ref,
+        d_send,
+        d_recv,
+        dsq_send,
+        dsq_recv,
+        h_all,
+        h_send,
+        e_send,
+        e_recv,
+    ) = refs[27:]
+    (
+        qd_v,
+        ld_v,
+        rd_v,
+        qc_v,
+        qr_v,
+        ka_v,
+        lat_v,
+        rot_v,
+        va_v,
+        ow_v,
+        gate_v,
+        up_v,
+        down_v,
+    ) = vmem
+    kv = lax.axis_index("kv")
+    tp = lax.axis_index("tp")
+    model_width = block_width * n_kv
+
+    loads = []
+    for index, (source, target) in enumerate(zip(hbm, vmem)):
+        if index in (10, 11):
+            target = target.at[:, pl.ds(0, hidden_width)]
+        elif index == 12:
+            target = target.at[pl.ds(0, hidden_width)]
+        copy = pltpu.make_async_copy(source, target, load_sems.at[index])
+        copy.start()
+        loads.append(copy)
+
+    barrier = pltpu.get_barrier_semaphore()
+    for d in range(1, n_tp):
+        pl.semaphore_signal(
+            barrier, inc=1, device_id=(kv, lax.rem(tp + d, n_tp)), device_id_type=MESH
+        )
+    for d in range(1, n_kv):
+        pl.semaphore_signal(
+            barrier, inc=1, device_id=(lax.rem(kv + d, n_kv), tp), device_id_type=MESH
+        )
+
+    sent = []
+
+    def send(axis, stage, d, source, target):
+        if axis == "tp":
+            peer, sems = (kv, lax.rem(tp + d, n_tp)), tp_sems
+        else:
+            peer, sems = (lax.rem(kv + d, n_kv), tp), kv_sems
+        copy = pltpu.make_async_remote_copy(
+            src_ref=source,
+            dst_ref=target,
+            send_sem=sems.at[stage, 0, d - 1],
+            recv_sem=sems.at[stage, 1, d - 1],
+            device_id=peer,
+            device_id_type=MESH,
+        )
+        copy.start()
+        sent.append(copy)
+        return copy
+
+    def arrive(copies):
+        for copy in copies:
+            copy.wait_recv()
+
+    pad = gate_v.shape[1] - hidden_width
+    if pad:
+        gate_v[:, hidden_width:] = jnp.zeros((block_width, pad), gate_v.dtype)
+        up_v[:, hidden_width:] = jnp.zeros((block_width, pad), up_v.dtype)
+        down_v[hidden_width:, :] = jnp.zeros((pad, block_width), down_v.dtype)
+
+    stream_f = stream_ref[...].astype(jnp.float32)
+    first_scaled = (stream_f * attention_gain[...]).astype(jnp.bfloat16)
+    for index in range(3):
+        loads[index].wait()
+    parts = [matmul(first_scaled, qd_v[...]), matmul(first_scaled, ld_v[...])]
+    rotary_part = matmul(first_scaled, rd_v[...])
+    square = jnp.sum(stream_f * stream_f, axis=1, keepdims=True)
+    last = jnp.concatenate(
+        [rotary_part, jnp.broadcast_to(square, (rows, LANES - rope))], axis=1
+    )
+    tiles = []
+    for part in parts:
+        for j in range(part.shape[1] // LANES):
+            tiles.append(part[:, j * LANES : (j + 1) * LANES])
+    tiles.append(last)
+    row_tiles = rows // SUBLANES
+    blocks = a_send.shape[1]
+    per_kv = blocks // n_kv
+    for t in range(n_tp):
+        for i in range(blocks):
+            k, r = divmod(i, row_tiles)
+            j = k * n_tp + t
+            if j < len(tiles):
+                a_send[t, i] = tiles[j][r * SUBLANES : (r + 1) * SUBLANES]
+            else:
+                a_send[t, i] = jnp.zeros((SUBLANES, LANES), jnp.float32)
+    pl.semaphore_wait(barrier, n_tp - 1 + n_kv - 1)
+    copies = [
+        send("tp", 1, d, a_send.at[lax.rem(tp + d, n_tp)], a_recv.at[tp]) for d in range(1, n_tp)
+    ]
+    stream_copies = [send("tp", 0, d, stream_ref, stream_all.at[tp]) for d in range(1, n_tp)]
+    stream_all[tp] = stream_ref[...]
+    a_recv[tp] = a_send[tp]
+    arrive(copies)
+    total = a_recv[0]
+    for t in range(1, n_tp):
+        total = total + a_recv[t]
+    a_sum[...] = total
+    copies = [
+        send(
+            "kv",
+            0,
+            d,
+            a_sum.at[pl.ds(lax.rem(kv + d, n_kv) * per_kv, per_kv)],
+            a_part.at[kv],
+        )
+        for d in range(1, n_kv)
+    ]
+    a_part[kv] = a_sum[pl.ds(kv * per_kv, per_kv)]
+    arrive(copies)
+    total = a_part[0]
+    for p in range(1, n_kv):
+        total = total + a_part[p]
+    a_total[pl.ds(kv * per_kv, per_kv)] = total
+    mine = a_total.at[pl.ds(kv * per_kv, per_kv)]
+    arrive([send("kv", 1, d, mine, mine) for d in range(1, n_kv)])
+    copies = [send("tp", 2, d, a_total, a_all.at[tp]) for d in range(1, n_tp)]
+    a_all[tp] = a_total[...]
+    arrive(copies)
+
+    def tile_of(j):
+        k, t = divmod(j, n_tp)
+        return jnp.concatenate([a_all[t, k * row_tiles + r] for r in range(row_tiles)], axis=0)
+
+    q_tiles, l_tiles = qrank // LANES, kvrank // LANES
+    last = tile_of(q_tiles + l_tiles)
+    first_scale = lax.rsqrt(last[:, rope : rope + 1] / model_width + epsilon)
+    query_low = first_scale * jnp.concatenate([tile_of(j) for j in range(q_tiles)], axis=1)
+    latent_new = first_scale * jnp.concatenate(
+        [tile_of(q_tiles + j) for j in range(l_tiles)], axis=1
+    )
+
+    def normed(values, gain):
+        mean = jnp.sum(values * values, axis=1, keepdims=True) / values.shape[1]
+        return (values * lax.rsqrt(mean + epsilon) * gain).astype(jnp.bfloat16)
+
+    query_normed = normed(query_low, query_gain[...])
+    latent_row = normed(latent_new, latent_gain[...]).astype(jnp.float32)
+    lane = lax.broadcasted_iota(jnp.int32, (rows, LANES), 1)
+    cosine, sine = cos_ref[...], sin_ref[...]
+    rotary_row = turned(first_scale * last, cosine[:, :LANES], sine[:, :LANES], rope)
+    rotary_row = jnp.where(lane < rope, rotary_row, 0.0).astype(jnp.bfloat16).astype(jnp.float32)
+
+    loads[3].wait()
+    query_plain = matmul(query_normed, qc_v[...]).astype(jnp.bfloat16)
+    loads[4].wait()
+    query_turned = turned(matmul(query_normed, qr_v[...]), cosine, sine, rope)
+    query_turned = query_turned.astype(jnp.bfloat16).astype(jnp.float32)
+    loads[5].wait()
+    scale = (nope + rope) ** (-0.5)
+    per_tile = LANES // rope
+    for h in range(heads):
+        row = pl.ds(h, rows, stride=heads)
+        latent = matmul(query_plain[:, h * nope : (h + 1) * nope], ka_v[h])
+        latent = latent.astype(jnp.bfloat16).astype(jnp.float32)
+        tile = h // per_tile
+        rotary = query_turned[:, tile * LANES : (tile + 1) * LANES]
+        shift = (h % per_tile) * rope
+        if shift:
+            rotary = pltpu.roll(rotary, LANES - shift, 1)
+        rotary = jnp.where(lane < rope, rotary, 0.0)
+        own = (
+            jnp.sum(latent * latent_row, axis=1, keepdims=True)
+            + jnp.sum(rotary * rotary_row, axis=1, keepdims=True)
+        ) * scale
+        for c in range(l_tiles):
+            q_lat[c, row, :] = latent[:, c * LANES : (c + 1) * LANES]
+            own_lat[c, row, :] = latent_row[:, c * LANES : (c + 1) * LANES]
+        q_rot[row, :] = rotary
+        own_stat[row, :] = jnp.broadcast_to(own, (rows, LANES))
+
+    group = SUBLANES // heads
+    steps = rows // group
+    unroll = 3 if steps % 3 == 0 else 1
+    sub_row = lax.broadcasted_iota(jnp.int32, (SUBLANES, 1), 0) // heads
+    loads[6].wait()
+    loads[7].wait()
+
+    def score_step(outer, carry):
+        for inner in range(unroll):
+            i = outer * unroll + inner
+            at = pl.ds(pl.multiple_of(i * SUBLANES, SUBLANES), SUBLANES)
+            query = jnp.concatenate([q_lat[c, at, :] for c in range(l_tiles)], axis=1).astype(
+                jnp.bfloat16
+            )
+            rotary = q_rot[at, :][:, :rope].astype(jnp.bfloat16)
+            result = None
+            for s in range(group):
+                b = i * group + s
+                score = matmul_nt(query, lat_v[b]) + matmul_nt(rotary, rot_v[b])
+                result = score if s == 0 else jnp.where(sub_row == s, score, result)
+            s_ref[at, :] = result * scale
+        return carry
+
+    lax.fori_loop(0, steps // unroll, score_step, 0)
+    scores = s_ref[...]
+    maxima = jnp.max(scores, axis=1, keepdims=True)
+    expo = jnp.exp(scores - maxima)
+    totals = jnp.sum(expo, axis=1, keepdims=True)
+    e_ref[...] = expo
+    all_rows = rows * heads
+    own_rows_count = all_rows // n_kv
+    stat_lane = lax.broadcasted_iota(jnp.int32, (all_rows, LANES), 1)
+    stats = jnp.where(stat_lane < LANES // 2, maxima, totals)
+    for p in range(n_kv):
+        st_send[p] = stats[p * own_rows_count : (p + 1) * own_rows_count]
+    stat_copies = [
+        send("kv", 2, d, st_send.at[lax.rem(kv + d, n_kv)], st_recv.at[kv])
+        for d in range(1, n_kv)
+    ]
+    st_recv[kv] = st_send[kv]
+
+    def weight_step(outer, carry):
+        for inner in range(unroll):
+            i = outer * unroll + inner
+            at = pl.ds(pl.multiple_of(i * SUBLANES, SUBLANES), SUBLANES)
+            weights = e_ref[at, :].astype(jnp.bfloat16)
+            result = None
+            for s in range(group):
+                value = matmul(weights, lat_v[i * group + s])
+                result = value if s == 0 else jnp.where(sub_row == s, value, result)
+            w_ref[at, :] = result
+        return carry
+
+    lax.fori_loop(0, steps // unroll, weight_step, 0)
+    for p in range(n_kv):
+        own = slice(p * own_rows_count, (p + 1) * own_rows_count)
+        w_send[p] = w_ref[own, :].astype(jnp.bfloat16)
+        for c in range(l_tiles):
+            own_rows[p, :, c * LANES : (c + 1) * LANES] = own_lat[c, own, :]
+        own_rows[p, :, kvrank:] = own_stat[own, :]
+    copies = [
+        send("kv", 3, d, w_send.at[lax.rem(kv + d, n_kv)], w_recv.at[kv]) for d in range(1, n_kv)
+    ]
+    w_recv[kv] = w_send[kv]
+    own = own_rows[kv]
+    own_score = own[:, kvrank : kvrank + 1]
+    arrive(stat_copies)
+    stat = [st_recv[p] for p in range(n_kv)]
+    largest = own_score
+    for p in range(n_kv):
+        largest = jnp.maximum(largest, stat[p][:, 0:1])
+    own_weight = jnp.exp(own_score - largest)
+    denominator = own_weight
+    factors = []
+    for p in range(n_kv):
+        factor = jnp.exp(stat[p][:, 0:1] - largest)
+        factors.append(factor)
+        denominator = denominator + factor * stat[p][:, LANES // 2 : LANES // 2 + 1]
+    arrive(copies)
+    merged = own_weight * own[:, :kvrank]
+    for p in range(n_kv):
+        merged = merged + factors[p] * w_recv[p].astype(jnp.float32)
+    latent_mix = (merged / denominator).astype(jnp.bfloat16)
+    loads[8].wait()
+    head_row = lax.rem(lax.broadcasted_iota(jnp.int32, (own_rows_count, 1), 0), heads)
+    values = None
+    for h in range(heads):
+        value = matmul(latent_mix, va_v[h])
+        values = value if h == 0 else jnp.where(head_row == h, value, values)
+    values = values.astype(jnp.bfloat16).astype(jnp.float32)
+    hv_send[...] = values
+    copies = [send("kv", 4, d, hv_send, hv_recv.at[kv]) for d in range(1, n_kv)]
+    hv_recv[kv] = values
+    arrive(copies)
+    for p in range(n_kv):
+        hv_rows[p * own_rows_count : (p + 1) * own_rows_count, :] = hv_recv[p]
+    head_f = jnp.concatenate(
+        [hv_rows[pl.ds(h, rows, stride=heads), :] for h in range(heads)], axis=1
+    )
+    head_square = jnp.sum(head_f * head_f, axis=1, keepdims=True)
+    head_scaled = (head_f * head_gain[...]).astype(jnp.bfloat16)
+    osq_send[...] = jnp.broadcast_to(head_square, (rows, LANES))
+    square_copies = [send("tp", 3, d, osq_send, osq_recv.at[tp]) for d in range(1, n_tp)]
+    osq_recv[tp] = osq_send[...]
+    loads[9].wait()
+    o_send[...] = matmul(head_scaled, ow_v[...]).astype(jnp.bfloat16)
+    copies = [send("tp", 4, d, o_send, o_recv.at[tp]) for d in range(1, n_tp)]
+    o_recv[tp] = o_send[...]
+    arrive(stream_copies)
+    stream_block = jnp.concatenate([stream_all[t] for t in range(n_tp)], axis=1).astype(
+        jnp.float32
+    )
+    arrive(square_copies)
+    square = osq_recv[0]
+    for t in range(1, n_tp):
+        square = square + osq_recv[t]
+    head_scale = lax.rsqrt(square[:, 0:1] / (heads * vdim * n_tp) + epsilon)
+    arrive(copies)
+    attended = o_recv[0].astype(jnp.float32)
+    for t in range(1, n_tp):
+        attended = attended + o_recv[t].astype(jnp.float32)
+    middle = (stream_block + head_scale * attended).astype(jnp.bfloat16).astype(jnp.float32)
+    for t in range(n_tp):
+        mid_ref[t] = middle[:, t * share : (t + 1) * share]
+
+    dsq_send[...] = jnp.broadcast_to(
+        jnp.sum(middle * middle, axis=1, keepdims=True), (rows, LANES)
+    )
+    square_copies = [send("kv", 5, d, dsq_send, dsq_recv.at[kv]) for d in range(1, n_kv)]
+    dsq_recv[kv] = dsq_send[...]
+    second_scaled = (middle * mixer_gain[...]).astype(jnp.bfloat16)
+    loads[10].wait()
+    loads[11].wait()
+    chunk = gate_v.shape[1] // n_kv
+    copies = []
+    for d in list(range(1, n_kv)) + [0]:
+        peer = lax.rem(kv + d, n_kv)
+        columns = pl.ds(pl.multiple_of(peer * chunk, LANES), chunk)
+        gate = matmul(second_scaled, gate_v[:, columns]).astype(jnp.bfloat16)
+        up = matmul(second_scaled, up_v[:, columns]).astype(jnp.bfloat16)
+        if d:
+            d_send[peer, :, :chunk] = gate
+            d_send[peer, :, chunk:] = up
+            copies.append(send("kv", 6, d, d_send.at[peer], d_recv.at[kv]))
+        else:
+            d_recv[kv, :, :chunk] = gate
+            d_recv[kv, :, chunk:] = up
+    arrive(square_copies)
+    square = dsq_recv[0]
+    for p in range(1, n_kv):
+        square = square + dsq_recv[p]
+    second_scale = lax.rsqrt(square[:, 0:1] / model_width + epsilon)
+    arrive(copies)
+    total = d_recv[0].astype(jnp.float32)
+    for p in range(1, n_kv):
+        total = total + d_recv[p].astype(jnp.float32)
+    gate = second_scale * total[:, :chunk]
+    up = second_scale * total[:, chunk:]
+    h_send[...] = (gate / (1.0 + jnp.exp(-gate)) * up).astype(jnp.bfloat16)
+    copies = [send("kv", 7, d, h_send, h_all.at[kv]) for d in range(1, n_kv)]
+    loads[12].wait()
+    mixed = matmul(h_send[...], down_v[pl.ds(pl.multiple_of(kv * chunk, LANES), chunk), :])
+    for d in range(1, n_kv):
+        copies[d - 1].wait_recv()
+        peer = lax.rem(kv + n_kv - d, n_kv)
+        mixed = mixed + matmul(
+            h_all[peer], down_v[pl.ds(pl.multiple_of(peer * chunk, LANES), chunk), :]
+        )
+    for t in range(n_tp):
+        e_send[t] = mixed[:, t * share : (t + 1) * share].astype(jnp.bfloat16)
+    copies = [
+        send("tp", 5, d, e_send.at[lax.rem(tp + d, n_tp)], e_recv.at[tp]) for d in range(1, n_tp)
+    ]
+    e_recv[tp] = e_send[tp]
+    arrive(copies)
+    total = e_recv[0].astype(jnp.float32)
+    for t in range(1, n_tp):
+        total = total + e_recv[t].astype(jnp.float32)
+    out_ref[...] = (mid_ref[tp] + total).astype(jnp.bfloat16)
+    for copy in sent:
+        copy.wait_send()
+
+
+def layer(
+    n_kv,
+    n_tp,
+    stream,
+    attention_gain,
+    query_down,
+    latent_down,
+    rotary_down,
+    query_gain,
+    latent_gain,
+    query_content,
+    query_rotary,
+    key_absorb,
+    value_absorb,
+    latent_cache,
+    rotary_cache,
+    head_gain,
+    output_weight,
+    mixer_gain,
+    gate_weight,
+    up_weight,
+    down_weight,
+):
+    rows, share = stream.shape
+    heads, nope, kvrank = key_absorb.shape
+    vdim = value_absorb.shape[2]
+    qrank = query_down.shape[1]
+    rope = rotary_down.shape[1]
+    positions = latent_cache.shape[1]
+    block_width, hidden_width = gate_weight.shape
+    aligned = (
+        all(
+            size % LANES == 0
+            for size in (share, qrank, kvrank, nope, vdim, positions, hidden_width)
+        )
+        and rope < LANES
+        and LANES % rope == 0
+        and (heads * rope) % LANES == 0
+        and rows % SUBLANES == 0
+        and SUBLANES % heads == 0
+        and rows % (SUBLANES // heads) == 0
+        and rows % n_kv == 0
+        and n_kv > 1
+        and n_tp > 1
+    )
+    if not aligned:
+        return local(
+            stream,
+            attention_gain,
+            query_down,
+            latent_down,
+            rotary_down,
+            query_gain,
+            latent_gain,
+            query_content,
+            query_rotary,
+            key_absorb,
+            value_absorb,
+            latent_cache,
+            rotary_cache,
+            head_gain,
+            output_weight,
+            mixer_gain,
+            gate_weight,
+            up_weight,
+            down_weight,
+        )
+    dims = (rows, share, qrank, kvrank, rope, nope, vdim, heads, hidden_width, block_width, share, positions)
+    cosine, sine = tables(rope, heads, positions * n_kv)
+    n_tiles = qrank // LANES + kvrank // LANES + 1
+    blocks = ceil_div(ceil_div(n_tiles, n_tp) * (rows // SUBLANES), n_kv) * n_kv
+    chunk = ceil_div(ceil_div(hidden_width, LANES), n_kv) * LANES
+    all_rows = rows * heads
+    own = all_rows // n_kv
+    l_tiles = kvrank // LANES
+    bf16, f32 = jnp.bfloat16, jnp.float32
+    big = (
+        query_down,
+        latent_down,
+        rotary_down,
+        query_content,
+        query_rotary,
+        key_absorb,
+        latent_cache,
+        rotary_cache,
+        value_absorb,
+        output_weight,
+        gate_weight,
+        up_weight,
+        down_weight,
+    )
+    held = [pltpu.VMEM(array.shape, array.dtype) for array in big]
+    held[10] = held[11] = pltpu.VMEM((block_width, chunk * n_kv), bf16)
+    held[12] = pltpu.VMEM((chunk * n_kv, block_width), bf16)
+    scratch = held + [
+        pltpu.SemaphoreType.DMA((len(big),)),
+        pltpu.SemaphoreType.DMA((6, 2, n_tp - 1)),
+        pltpu.SemaphoreType.DMA((8, 2, n_kv - 1)),
+        pltpu.VMEM((n_tp, rows, share), bf16),
+        pltpu.VMEM((n_tp, blocks, SUBLANES, LANES), f32),
+        pltpu.VMEM((n_tp, blocks, SUBLANES, LANES), f32),
+        pltpu.VMEM((blocks, SUBLANES, LANES), f32),
+        pltpu.VMEM((n_kv, blocks // n_kv, SUBLANES, LANES), f32),
+        pltpu.VMEM((blocks, SUBLANES, LANES), f32),
+        pltpu.VMEM((n_tp, blocks, SUBLANES, LANES), f32),
+        pltpu.VMEM((l_tiles, all_rows, LANES), f32),
+        pltpu.VMEM((all_rows, LANES), f32),
+        pltpu.VMEM((l_tiles, all_rows, LANES), f32),
+        pltpu.VMEM((all_rows, LANES), f32),
+        pltpu.VMEM((n_kv, own, kvrank + LANES), f32),
+        pltpu.VMEM((all_rows, positions), f32),
+        pltpu.VMEM((all_rows, positions), f32),
+        pltpu.VMEM((all_rows, kvrank), f32),
+        pltpu.VMEM((n_kv, own, kvrank), bf16),
+        pltpu.VMEM((n_kv, own, kvrank), bf16),
+        pltpu.VMEM((n_kv, own, LANES), f32),
+        pltpu.VMEM((n_kv, own, LANES), f32),
+        pltpu.VMEM((own, vdim), f32),
+        pltpu.VMEM((n_kv, own, vdim), f32),
+        pltpu.VMEM((all_rows, vdim), f32),
+        pltpu.VMEM((n_tp, rows, block_width), bf16),
+        pltpu.VMEM((n_tp, rows, LANES), f32),
+        pltpu.VMEM((rows, block_width), bf16),
+        pltpu.VMEM((rows, LANES), f32),
+        pltpu.VMEM((n_tp, rows, share), f32),
+        pltpu.VMEM((n_kv, rows, 2 * chunk), bf16),
+        pltpu.VMEM((n_kv, rows, 2 * chunk), bf16),
+        pltpu.VMEM((rows, LANES), f32),
+        pltpu.VMEM((n_kv, rows, LANES), f32),
+        pltpu.VMEM((n_kv, rows, chunk), bf16),
+        pltpu.VMEM((rows, chunk), bf16),
+        pltpu.VMEM((n_tp, rows, share), bf16),
+        pltpu.VMEM((n_tp, rows, share), bf16),
+    ]
+    vmem = pl.BlockSpec(memory_space=pltpu.VMEM)
+    return pl.pallas_call(
+        functools.partial(fused, n_kv, n_tp, dims),
+        out_shape=jax.ShapeDtypeStruct(stream.shape, stream.dtype),
+        in_specs=[vmem] * 8 + [pl.BlockSpec(memory_space=pl.ANY)] * len(big),
+        out_specs=vmem,
+        scratch_shapes=scratch,
+        compiler_params=pltpu.CompilerParams(
+            collective_id=0, has_side_effects=True, vmem_limit_bytes=64000000
+        ),
+        name="layer",
+    )(
+        stream,
+        attention_gain[None],
+        query_gain[None],
+        latent_gain[None],
+        head_gain[None],
+        mixer_gain[None],
+        cosine,
+        sine,
+        *big,
+    )
+
+
 def solution(mesh):
     return jax.shard_map(
-        local,
+        functools.partial(layer, mesh.shape["kv"], mesh.shape["tp"]),
         mesh=mesh,
         in_specs=(
             P(None, ("kv", "tp")),

time: 367 us -> 69 us (0.19)
  blocking collectives: 170 us -> 0 us
  waiting for transfers between devices: 144 us -> 0 us
  Pallas kernels: 0 us -> 62.1 us
  matrix products: 24.1 us -> 0 us
  between operations: 13.2 us -> 0.01 us
  other arithmetic: 10.1 us -> 0 us
    psum x2 -> x0, waiting for transfers between devices: 125 us -> none  [the longest x1 75 us: local(): lax.psum((matmul(first_scaled, query_down), matmul(first_scaled, latent_d...]
    all_gather x4 -> x0, blocking collectives: 95.1 us -> none  [the longest x1 32.5 us: local(): lax.all_gather(weighted[None], 'kv', axis=0, tiled=True).astype(jnp.float32)]
    psum x4 -> x0, blocking collectives: 75.2 us -> none  [the longest x1 40.5 us: local(): lax.psum((matmul(first_scaled, query_down), matmul(first_scaled, latent_d...]
    pallas_call x0 -> x1, Pallas kernels: none -> 62.1 us  [layer(): pl.pallas_call(functools.partial(fused, n_kv, n_tp, dims), out_shape=jax....]
    dot_general x14 -> x0, matrix products: 24.1 us -> none  [the longest x9 13 us: matmul(): return jnp.dot(left, right, preferred_element_type=jnp.float32)]
    unnamed x4 -> x0, waiting for transfers between devices: 19.1 us -> none
    reduce_sum x8 -> x0, other arithmetic: 5.24 us -> none  [the longest x2 1.89 us: sum_squares(): return jnp.sum(values * values, axis=-1)]
  transfers between devices with their start and end apart: 3 -> 0, of which waited for: 3 -> 0; matrix products, arithmetic and copies ran while one was open for 2% -> 0% of each run, Pallas kernels for 0% -> 0%
where the time goes in v1:
time: 69 us; the launch traced here: 68.6 us
  Pallas kernels  62.1 us (90%)
  local copies, waits for them, and re-layouts  6.47 us (9%)
    pallas_call x1, Pallas kernels, layer(): pl.pallas_call(functools.partial(fused, n_kv, n_tp, dims), out_shape=jax....  62.1 us
    unnamed x3, local copies, waits for them, and re-layouts  5.17 us

profile of v1, /device:TPU:0, one launch (start us, length us, event | category | flops | bytes accessed | tf_op | source)
XLA Modules:
  0.0 68.6 jit_solution(10590629480450368295)
XLA Ops:
  0.0 1.3 %broadcast_in_dim.16.query_gain = f32[1,1536]{1,0:T(1,128)} reshape(f32[1536]{0:T(1024)} %param.26) | data formatting | bytes 12288 | tf_op jit(solution)/shard_map/broadcast_in_dim | solution.py:768
  1.3 1.4 %copy.22.refs_2_ = bf16[128,64]{1,0:T(8,128)(2,1)} copy(bf16[128,64]{0,1:T(8,128)(2,1)} %param.25) | data formatting | bytes 32768 | tf_op args[4]
  2.7 2.5 %copy.23.refs_7_ = bf16[24,256,64]{2,1,0:T(8,128)(2,1)} copy(bf16[24,256,64]{1,2,0:T(8,128)(2,1)} %param.33) | data formatting | bytes 1572864 | tf_op args[12]
  5.2 62.1 %layer.1 = bf16[24,128]{1,0:T(8,128)(2,1)} custom-call(bf16[24,128]{1,0:T(8,128)(2,1)} %stream_ref.1, f32[1,128]{1,0:T(1,128)} %bitcast.7, f32[1,1536]{1,0:T(1,128)} %broadcast_in_dim.16.query_gain, f32[1,512]{1,0:T(1,128)} %bitcast.4, f32[1,512]{1,0:T(1,128)} %bitcast.5, f32[1,512]{1,0:T(1,128)} %bitcast.6, f32[1,256]{1,0:T(1,128)} %constant.4.clone.cos_ref, ...), custom_call_target="tpu_custom_call" | custom-call | tf_op jit(solution)/shard_map/layer/pallas_call | solution.py:755
  67.3 1.3 %copy.25 = bf16[24,128]{1,0:T(8,128)(2,1)} copy(bf16[24,128]{1,0:T(8,128)(2,1)} %layer.1) | data formatting | bytes 12288

commit v2 on v1

--- a/solution.py
+++ b/solution.py
@@ -189,6 +189,17 @@
     behind = pltpu.roll(values, half, 1)
     swapped = jnp.where(lax.rem(lane, width) < half, ahead, behind)
     return values * cosine + swapped * sine
+
+
+def split_sum(values, lanes):
+    high = values.astype(jnp.bfloat16).astype(jnp.float32)
+    lane = lax.broadcasted_iota(jnp.int32, (values.shape[0], lanes), 1)
+    return jnp.where(lane < lanes // 2, high, values - high).astype(jnp.bfloat16)
+
+
+def joined_sum(parts, lanes):
+    half = lanes // 2
+    return parts[:, 0:1] + parts[:, half : half + 1]
 
 
 def matmul_nt(left, right):
@@ -242,14 +253,10 @@
         hv_recv,
         hv_rows,
         o_recv,
-        osq_recv,
         o_send,
-        osq_send,
         mid_ref,
         d_send,
         d_recv,
-        dsq_send,
-        dsq_recv,
         h_all,
         h_send,
         e_send,
@@ -328,7 +335,7 @@
     for index in range(3):
         loads[index].wait()
     parts = [matmul(first_scaled, qd_v[...]), matmul(first_scaled, ld_v[...])]
-    rotary_part = matmul(first_scaled, rd_v[...])
+    rotary_part = matmul_nt(first_scaled, rd_v[...])
     square = jnp.sum(stream_f * stream_f, axis=1, keepdims=True)
     last = jnp.concatenate(
         [rotary_part, jnp.broadcast_to(square, (rows, LANES - rope))], axis=1
@@ -346,21 +353,19 @@
             k, r = divmod(i, row_tiles)
             j = k * n_tp + t
             if j < len(tiles):
-                a_send[t, i] = tiles[j][r * SUBLANES : (r + 1) * SUBLANES]
+                a_send[t, i] = tiles[j][r * SUBLANES : (r + 1) * SUBLANES].astype(jnp.bfloat16)
             else:
-                a_send[t, i] = jnp.zeros((SUBLANES, LANES), jnp.float32)
+                a_send[t, i] = jnp.zeros((SUBLANES, LANES), jnp.bfloat16)
     pl.semaphore_wait(barrier, n_tp - 1 + n_kv - 1)
     copies = [
         send("tp", 1, d, a_send.at[lax.rem(tp + d, n_tp)], a_recv.at[tp]) for d in range(1, n_tp)
     ]
-    stream_copies = [send("tp", 0, d, stream_ref, stream_all.at[tp]) for d in range(1, n_tp)]
-    stream_all[tp] = stream_ref[...]
     a_recv[tp] = a_send[tp]
     arrive(copies)
-    total = a_recv[0]
+    total = a_recv[0].astype(jnp.float32)
     for t in range(1, n_tp):
-        total = total + a_recv[t]
-    a_sum[...] = total
+        total = total + a_recv[t].astype(jnp.float32)
+    a_sum[...] = total.astype(jnp.bfloat16)
     copies = [
         send(
             "kv",
@@ -371,12 +376,14 @@
         )
         for d in range(1, n_kv)
     ]
+    stream_copies = [send("tp", 0, d, stream_ref, stream_all.at[tp]) for d in range(1, n_tp)]
+    stream_all[tp] = stream_ref[...]
     a_part[kv] = a_sum[pl.ds(kv * per_kv, per_kv)]
     arrive(copies)
-    total = a_part[0]
+    total = a_part[0].astype(jnp.float32)
     for p in range(1, n_kv):
-        total = total + a_part[p]
-    a_total[pl.ds(kv * per_kv, per_kv)] = total
+        total = total + a_part[p].astype(jnp.float32)
+    a_total[pl.ds(kv * per_kv, per_kv)] = total.astype(jnp.bfloat16)
     mine = a_total.at[pl.ds(kv * per_kv, per_kv)]
     arrive([send("kv", 1, d, mine, mine) for d in range(1, n_kv)])
     copies = [send("tp", 2, d, a_total, a_all.at[tp]) for d in range(1, n_tp)]
@@ -385,7 +392,7 @@
 
     def tile_of(j):
         k, t = divmod(j, n_tp)
-        return jnp.concatenate([a_all[t, k * row_tiles + r] for r in range(row_tiles)], axis=0)
+        return jnp.concatenate([a_all[t, k * row_tiles + r].astype(jnp.float32) for r in range(row_tiles)], axis=0)
 
     q_tiles, l_tiles = qrank // LANES, kvrank // LANES
     last = tile_of(q_tiles + l_tiles)
@@ -399,7 +406,8 @@
         mean = jnp.sum(values * values, axis=1, keepdims=True) / values.shape[1]
         return (values * lax.rsqrt(mean + epsilon) * gain).astype(jnp.bfloat16)
 
-    query_normed = normed(query_low, query_gain[...])
+    gain = jnp.concatenate([query_gain[j : j + 1] for j in range(q_tiles)], axis=1)
+    query_normed = normed(query_low, gain)
     latent_row = normed(latent_new, latent_gain[...]).astype(jnp.float32)
     lane = lax.broadcasted_iota(jnp.int32, (rows, LANES), 1)
     cosine, sine = cos_ref[...], sin_ref[...]
@@ -452,7 +460,7 @@
             result = None
             for s in range(group):
                 b = i * group + s
-                score = matmul_nt(query, lat_v[b]) + matmul_nt(rotary, rot_v[b])
+                score = matmul_nt(query, lat_v[b]) + matmul(rotary, rot_v[b])
                 result = score if s == 0 else jnp.where(sub_row == s, score, result)
             s_ref[at, :] = result * scale
         return carry
@@ -523,75 +531,67 @@
     for h in range(heads):
         value = matmul(latent_mix, va_v[h])
         values = value if h == 0 else jnp.where(head_row == h, value, values)
-    values = values.astype(jnp.bfloat16).astype(jnp.float32)
+    values = values.astype(jnp.bfloat16)
     hv_send[...] = values
     copies = [send("kv", 4, d, hv_send, hv_recv.at[kv]) for d in range(1, n_kv)]
     hv_recv[kv] = values
     arrive(copies)
     for p in range(n_kv):
-        hv_rows[p * own_rows_count : (p + 1) * own_rows_count, :] = hv_recv[p]
+        hv_rows[p * own_rows_count : (p + 1) * own_rows_count, :] = hv_recv[p].astype(jnp.float32)
     head_f = jnp.concatenate(
         [hv_rows[pl.ds(h, rows, stride=heads), :] for h in range(heads)], axis=1
     )
     head_square = jnp.sum(head_f * head_f, axis=1, keepdims=True)
     head_scaled = (head_f * head_gain[...]).astype(jnp.bfloat16)
-    osq_send[...] = jnp.broadcast_to(head_square, (rows, LANES))
-    square_copies = [send("tp", 3, d, osq_send, osq_recv.at[tp]) for d in range(1, n_tp)]
-    osq_recv[tp] = osq_send[...]
     loads[9].wait()
-    o_send[...] = matmul(head_scaled, ow_v[...]).astype(jnp.bfloat16)
+    o_send[:, :block_width] = matmul(head_scaled, ow_v[...]).astype(jnp.bfloat16)
+    o_send[:, block_width:] = split_sum(head_square, LANES)
     copies = [send("tp", 4, d, o_send, o_recv.at[tp]) for d in range(1, n_tp)]
     o_recv[tp] = o_send[...]
     arrive(stream_copies)
     stream_block = jnp.concatenate([stream_all[t] for t in range(n_tp)], axis=1).astype(
         jnp.float32
     )
-    arrive(square_copies)
-    square = osq_recv[0]
-    for t in range(1, n_tp):
-        square = square + osq_recv[t]
-    head_scale = lax.rsqrt(square[:, 0:1] / (heads * vdim * n_tp) + epsilon)
     arrive(copies)
     attended = o_recv[0].astype(jnp.float32)
     for t in range(1, n_tp):
         attended = attended + o_recv[t].astype(jnp.float32)
+    square = joined_sum(attended[:, block_width:], LANES)
+    attended = attended[:, :block_width]
+    head_scale = lax.rsqrt(square / (heads * vdim * n_tp) + epsilon)
     middle = (stream_block + head_scale * attended).astype(jnp.bfloat16).astype(jnp.float32)
     for t in range(n_tp):
         mid_ref[t] = middle[:, t * share : (t + 1) * share]
 
-    dsq_send[...] = jnp.broadcast_to(
-        jnp.sum(middle * middle, axis=1, keepdims=True), (rows, LANES)
-    )
-    square_copies = [send("kv", 5, d, dsq_send, dsq_recv.at[kv]) for d in range(1, n_kv)]
-    dsq_recv[kv] = dsq_send[...]
+    square = split_sum(jnp.sum(middle * middle, axis=1, keepdims=True), LANES)
     second_scaled = (middle * mixer_gain[...]).astype(jnp.bfloat16)
     loads[10].wait()
     loads[11].wait()
     chunk = gate_v.shape[1] // n_kv
     copies = []
-    for d in list(range(1, n_kv)) + [0]:
+    far_first = sorted(range(1, n_kv), key=lambda d: abs(2 * d - n_kv)) + [0]
+    for d in far_first:
         peer = lax.rem(kv + d, n_kv)
         columns = pl.ds(pl.multiple_of(peer * chunk, LANES), chunk)
         gate = matmul(second_scaled, gate_v[:, columns]).astype(jnp.bfloat16)
         up = matmul(second_scaled, up_v[:, columns]).astype(jnp.bfloat16)
         if d:
             d_send[peer, :, :chunk] = gate
-            d_send[peer, :, chunk:] = up
+            d_send[peer, :, chunk : 2 * chunk] = up
+            d_send[peer, :, 2 * chunk :] = square
             copies.append(send("kv", 6, d, d_send.at[peer], d_recv.at[kv]))
         else:
             d_recv[kv, :, :chunk] = gate
-            d_recv[kv, :, chunk:] = up
-    arrive(square_copies)
-    square = dsq_recv[0]
-    for p in range(1, n_kv):
-        square = square + dsq_recv[p]
-    second_scale = lax.rsqrt(square[:, 0:1] / model_width + epsilon)
+            d_recv[kv, :, chunk : 2 * chunk] = up
+            d_recv[kv, :, 2 * chunk :] = square
     arrive(copies)
     total = d_recv[0].astype(jnp.float32)
     for p in range(1, n_kv):
         total = total + d_recv[p].astype(jnp.float32)
+    square = joined_sum(total[:, 2 * chunk :], LANES)
+    second_scale = lax.rsqrt(square / model_width + epsilon)
     gate = second_scale * total[:, :chunk]
-    up = second_scale * total[:, chunk:]
+    up = second_scale * total[:, chunk : 2 * chunk]
     h_send[...] = (gate / (1.0 + jnp.exp(-gate)) * up).astype(jnp.bfloat16)
     copies = [send("kv", 7, d, h_send, h_all.at[kv]) for d in range(1, n_kv)]
     loads[12].wait()
@@ -696,12 +696,12 @@
     big = (
         query_down,
         latent_down,
-        rotary_down,
+        rotary_down.T,
         query_content,
         query_rotary,
         key_absorb,
         latent_cache,
-        rotary_cache,
+        jnp.swapaxes(rotary_cache, 1, 2),
         value_absorb,
         output_weight,
         gate_weight,
@@ -716,12 +716,12 @@
         pltpu.SemaphoreType.DMA((6, 2, n_tp - 1)),
         pltpu.SemaphoreType.DMA((8, 2, n_kv - 1)),
         pltpu.VMEM((n_tp, rows, share), bf16),
-        pltpu.VMEM((n_tp, blocks, SUBLANES, LANES), f32),
-        pltpu.VMEM((n_tp, blocks, SUBLANES, LANES), f32),
-        pltpu.VMEM((blocks, SUBLANES, LANES), f32),
-        pltpu.VMEM((n_kv, blocks // n_kv, SUBLANES, LANES), f32),
-        pltpu.VMEM((blocks, SUBLANES, LANES), f32),
-        pltpu.VMEM((n_tp, blocks, SUBLANES, LANES), f32),
+        pltpu.VMEM((n_tp, blocks, SUBLANES, LANES), bf16),
+        pltpu.VMEM((n_tp, blocks, SUBLANES, LANES), bf16),
+        pltpu.VMEM((blocks, SUBLANES, LANES), bf16),
+        pltpu.VMEM((n_kv, blocks // n_kv, SUBLANES, LANES), bf16),
+        pltpu.VMEM((blocks, SUBLANES, LANES), bf16),
+        pltpu.VMEM((n_tp, blocks, SUBLANES, LANES), bf16),
         pltpu.VMEM((l_tiles, all_rows, LANES), f32),
         pltpu.VMEM((all_rows, LANES), f32),
         pltpu.VMEM((l_tiles, all_rows, LANES), f32),
@@ -734,18 +734,14 @@
         pltpu.VMEM((n_kv, own, kvrank), bf16),
         pltpu.VMEM((n_kv, own, LANES), f32),
         pltpu.VMEM((n_kv, own, LANES), f32),
-        pltpu.VMEM((own, vdim), f32),
-        pltpu.VMEM((n_kv, own, vdim), f32),
+        pltpu.VMEM((own, vdim), bf16),
+        pltpu.VMEM((n_kv, own, vdim), bf16),
         pltpu.VMEM((all_rows, vdim), f32),
-        pltpu.VMEM((n_tp, rows, block_width), bf16),
-        pltpu.VMEM((n_tp, rows, LANES), f32),
-        pltpu.VMEM((rows, block_width), bf16),
-        pltpu.VMEM((rows, LANES), f32),
+        pltpu.VMEM((n_tp, rows, block_width + LANES), bf16),
+        pltpu.VMEM((rows, block_width + LANES), bf16),
         pltpu.VMEM((n_tp, rows, share), f32),
-        pltpu.VMEM((n_kv, rows, 2 * chunk), bf16),
-        pltpu.VMEM((n_kv, rows, 2 * chunk), bf16),
-        pltpu.VMEM((rows, LANES), f32),
-        pltpu.VMEM((n_kv, rows, LANES), f32),
+        pltpu.VMEM((n_kv, rows, 2 * chunk + LANES), bf16),
+        pltpu.VMEM((n_kv, rows, 2 * chunk + LANES), bf16),
         pltpu.VMEM((n_kv, rows, chunk), bf16),
         pltpu.VMEM((rows, chunk), bf16),
         pltpu.VMEM((n_tp, rows, share), bf16),
@@ -765,7 +761,7 @@
     )(
         stream,
         attention_gain[None],
-        query_gain[None],
+        query_gain.reshape(qrank // LANES, LANES),
         latent_gain[None],
         head_gain[None],
         mixer_gain[None],

time: 69 us -> 60.2 us (0.87)
  local copies, waits for them, and re-layouts: 6.47 us -> 1.29 us
  Pallas kernels: 62.1 us -> 58.7 us
    unnamed x3 -> x1, local copies, waits for them, and re-layouts: 5.17 us -> 1.29 us
    pallas_call x1, Pallas kernels: 62.1 us -> 58.7 us  [layer(): pl.pallas_call(functools.partial(fused, n_kv, n_tp, dims), out_shape=jax....]
    broadcast_in_dim x1 -> x0, local copies, waits for them, and re-layouts: 1.29 us -> none  [layer(): query_gain[None]]
where the time goes in v2:
time: 60.2 us; the launch traced here: 60 us
  Pallas kernels  58.7 us (98%)
  local copies, waits for them, and re-layouts  1.29 us (2%)
    pallas_call x1, Pallas kernels, layer(): pl.pallas_call(functools.partial(fused, n_kv, n_tp, dims), out_shape=jax....  58.7 us
    unnamed x1, local copies, waits for them, and re-layouts  1.29 us

profile of v2, /device:TPU:0, one launch (start us, length us, event | category | flops | bytes accessed | tf_op | source)
XLA Modules:
  0.0 60.0 jit_solution(17672554624179757404)
XLA Ops:
  0.0 58.7 %layer.1 = bf16[24,128]{1,0:T(8,128)(2,1)} custom-call(bf16[24,128]{1,0:T(8,128)(2,1)} %stream_ref.1, f32[1,128]{1,0:T(1,128)} %bitcast.13, f32[12,128]{1,0:T(8,128)} %bitcast.9, f32[1,512]{1,0:T(1,128)} %bitcast.10, f32[1,512]{1,0:T(1,128)} %bitcast.11, f32[1,512]{1,0:T(1,128)} %bitcast.12, f32[1,256]{1,0:T(1,128)} %constant.4.clone.cos_ref, ...), custom_call_target="tpu_custom_call" | custom-call | tf_op jit(solution)/shard_map/layer/pallas_call | solution.py:751
  58.7 1.3 %copy.23 = bf16[24,128]{1,0:T(8,128)(2,1)} copy(bf16[24,128]{1,0:T(8,128)(2,1)} %layer.1) | data formatting | bytes 12288
